TPU v7x, 32 devices: a whole 2x2x4 slice. The times are simulated.
32 devices in a mesh: ep: 8 (over z, x), tp: 4 (over y, core).
Axes of the slice: x: 2, y: 2, z: 4, core: 2. Of those that a mesh axis runs over, the one named last changes fastest.
Arguments:
- layer_in: bfloat16 [128, 2048], P('ep'), may hold values from -6 to 6
- state_in: float32 [128, 32, 4096], P('ep', 'tp'), may hold values from -6 to 6
- mix_gain: float32 [2048], replicated, may hold values from 0.1 to 1.9
- rec_weight: bfloat16 [2048, 2048], P('ep', 'tp'), may hold values from -0.125 to 0.125
- key_weight: bfloat16 [2048, 2048], P('ep', 'tp'), may hold values from -0.125 to 0.125
- val_weight: bfloat16 [2048, 2048], P('ep', 'tp'), may hold values from -0.125 to 0.125
- decay_down: bfloat16 [2048, 64], replicated, may hold values from -0.125 to 0.125
- decay_up: bfloat16 [64, 2048], P(None, 'tp'), may hold values from -0.75 to 0.75
- decay_base: float32 [2048], P('tp'), may hold values from -6 to 6
- rate_down: bfloat16 [2048, 64], replicated, may hold values from -0.125 to 0.125
- rate_up: bfloat16 [64, 2048], P(None, 'tp'), may hold values from -0.75 to 0.75
- rate_base: float32 [2048], P('tp'), may hold values from -6 to 6
- key_scale: float32 [2048], P('tp'), may hold values from 0.25 to 4
- group_gain: float32 [2048], P('tp'), may hold values from 0.1 to 1.9
- out_weight: bfloat16 [2048, 2048], P('tp', 'ep'), may hold values from -0.125 to 0.125
- post_gain: float32 [2048], replicated, may hold values from 0.1 to 1.9
- ffn_gain: float32 [2048], replicated, may hold values from 0.1 to 1.9
- routes: int32 [128, 4], P('ep'), may hold values from 0 to 7, all different within a row; in each aligned block of 16 rows (0 to 15, 16 to 31, ...) at most 16 rows name the same one
- route_gates: float32 [128, 4], P('ep'), may hold values from 0.05 to 1
- expert_gate: bfloat16 [8, 2048, 2048], P('ep', None, 'tp'), may hold values from -0.375 to 0.375
- expert_up: bfloat16 [8, 2048, 2048], P('ep', None, 'tp'), may hold values from -0.375 to 0.375
- expert_down: bfloat16 [8, 2048, 2048], P('ep', 'tp'), may hold values from -0.125 to 0.125
- out_gain: float32 [2048], replicated, may hold values from 0.1 to 1.9
Outputs:
- layer_out: bfloat16 [128, 2048], P('ep')
- new_state: float32 [128, 32, 4096], P('ep', 'tp')
Inputs may be any that keep to these rules, and one draw needn't show every extreme that they name: `routes`: each row names 4 different experts. Within the rows of one device (aligned blocks of 16 rows) no expert is named by more than 16 rows, and in every draw some block names some expert exactly 16 times.
All inputs are finite; a program needn't handle non-finite values.
Results may differ from a plain program's by a relative error of at most 0.017.
Values may be sent and summed in bfloat16 or wider, within the bound.
A program may use at most 128 MiB of HBM per device.

v0:
```python
import jax
import jax.numpy as jnp
from jax import lax
from jax.sharding import PartitionSpec as P

HEAD_DIM = 64


norm_eps = 1e-06
group_eps = 0.00064
clamp_limit = 7.0
gate_alpha = 1.702


def rms_scale(values, scales):
    return values * lax.rsqrt(jnp.mean(values * values, axis=-1, keepdims=True) + norm_eps) * scales


def rounded(values):
    return lax.optimization_barrier(values.astype(jnp.bfloat16)).astype(jnp.float32)


def local(
    layer_in,
    state_in,
    mix_gain,
    rec_weight,
    key_weight,
    val_weight,
    decay_down,
    decay_up,
    decay_base,
    rate_down,
    rate_up,
    rate_base,
    key_scale,
    group_gain,
    out_weight,
    post_gain,
    ffn_gain,
    routes,
    route_gates,
    expert_gate,
    expert_up,
    expert_down,
    out_gain,
):
    seq_count = layer_in.shape[0]
    model_width = layer_in.shape[1]
    head_count = state_in.shape[1]
    local_cols = rec_weight.shape[1]
    normed_in = rms_scale(layer_in.astype(jnp.float32), mix_gain).astype(jnp.bfloat16)
    spread_rows = lax.all_to_all(normed_in, "ep", split_axis=1, concat_axis=0, tiled=True)
    joined = jnp.concatenate((rec_weight, key_weight, val_weight), axis=1)
    summed = lax.psum_scatter(
        jnp.dot(spread_rows, joined, preferred_element_type=jnp.float32),
        "ep",
        scatter_dimension=0,
        tiled=True,
    )
    rec_sum = summed[:, :local_cols]
    key_sum = summed[:, local_cols : 2 * local_cols]
    val_sum = summed[:, 2 * local_cols :]
    head_shape = (seq_count, head_count, HEAD_DIM)
    rec_rows = rounded(rec_sum).reshape(head_shape)
    key_rows = rounded(key_sum).reshape(head_shape)
    val_rows = rounded(val_sum).reshape(head_shape)
    decay_hidden = jnp.tanh(
        jnp.dot(normed_in, decay_down, preferred_element_type=jnp.float32)
    ).astype(jnp.bfloat16)
    rate_hidden = jnp.dot(normed_in, rate_down, preferred_element_type=jnp.float32).astype(
        jnp.bfloat16
    )
    decay_pre = decay_base + jnp.dot(decay_hidden, decay_up, preferred_element_type=jnp.float32)
    decay_factor = jnp.exp(-jnp.exp(-jax.nn.softplus(-decay_pre) - 0.5)).reshape(head_shape)
    learn_rate = jax.nn.sigmoid(
        rate_base + jnp.dot(rate_hidden, rate_up, preferred_element_type=jnp.float32)
    ).reshape(head_shape)
    scaled_key = key_rows * key_scale.reshape(head_count, HEAD_DIM)
    unit_key = scaled_key * lax.rsqrt(
        jnp.sum(scaled_key * scaled_key, axis=-1, keepdims=True) + norm_eps
    )
    old_state = state_in.reshape(seq_count, head_count, HEAD_DIM, HEAD_DIM)
    along_key = jnp.sum(old_state * unit_key[:, :, None, :], axis=-1)
    new_state = (
        old_state * decay_factor[:, :, None, :]
        - along_key[..., None] * (unit_key * learn_rate)[:, :, None, :]
        + val_rows[..., None] * (key_rows * learn_rate)[:, :, None, :]
    )
    readout = jnp.sum(new_state * rec_rows[:, :, None, :], axis=-1)
    centred = readout - jnp.mean(readout, axis=-1, keepdims=True)
    normed_out = centred * lax.rsqrt(
        jnp.mean(centred * centred, axis=-1, keepdims=True) + group_eps
    )
    normed_out = (
        (normed_out * group_gain.reshape(head_count, HEAD_DIM))
        .reshape(seq_count, local_cols)
        .astype(jnp.bfloat16)
    )
    head_partial = jnp.dot(
        normed_out,
        lax.all_gather(out_weight, "ep", axis=1, tiled=True),
        preferred_element_type=jnp.float32,
    )
    mix_sum = lax.psum(head_partial.astype(jnp.bfloat16), "tp").astype(jnp.float32)
    middle = (layer_in.astype(jnp.float32) + rms_scale(mix_sum, post_gain)).astype(jnp.bfloat16)
    ffn_in = rms_scale(middle.astype(jnp.float32), ffn_gain).astype(jnp.bfloat16)
    top_count = routes.shape[1]
    local_experts = expert_gate.shape[0]
    expert_total = lax.axis_size("ep") * local_experts
    capacity = max(2, 2 * seq_count * top_count // expert_total)
    slot_total = expert_total * capacity
    flat_routes = routes.reshape(-1)
    onehot = (flat_routes[:, None] == jnp.arange(expert_total, dtype=jnp.int32)[None, :]).astype(
        jnp.int32
    )
    slot_rank = jnp.sum((jnp.cumsum(onehot, axis=0) - 1) * onehot, axis=1)
    slot_index = flat_routes * capacity + slot_rank
    slot_range = jnp.arange(slot_total, dtype=jnp.int32)
    dispatch_table = jnp.sum(
        (slot_range[:, None] == slot_index[None, :])
        .astype(jnp.bfloat16)
        .reshape(slot_total, seq_count, top_count),
        axis=2,
    )
    send_rows = jnp.dot(dispatch_table, ffn_in, preferred_element_type=jnp.float32).astype(
        jnp.bfloat16
    )
    send_rows = send_rows.reshape(lax.axis_size("ep"), local_experts, capacity, model_width)
    arrived = lax.all_to_all(send_rows, "ep", split_axis=0, concat_axis=0, tiled=True)
    gate_cut = jnp.minimum(
        jnp.einsum("seid,edf->seif", arrived, expert_gate, preferred_element_type=jnp.float32),
        clamp_limit,
    )
    up_cut = jnp.clip(
        jnp.einsum("seid,edf->seif", arrived, expert_up, preferred_element_type=jnp.float32),
        -clamp_limit,
        clamp_limit,
    )
    hidden = ((up_cut + 1.0) * gate_cut * jax.nn.sigmoid(gate_alpha * gate_cut)).astype(
        jnp.bfloat16
    )
    partial_value = jnp.einsum(
        "seif,efd->seid", hidden, expert_down, preferred_element_type=jnp.float32
    )
    returned = lax.psum(partial_value.astype(jnp.bfloat16), "tp")
    back_rows = lax.all_to_all(returned, "ep", split_axis=0, concat_axis=0, tiled=True)
    back_flat = back_rows.reshape(slot_total, model_width)
    combine_table = (slot_index[:, None] == slot_range[None, :]).astype(jnp.bfloat16)
    picked = jnp.dot(combine_table, back_flat, preferred_element_type=jnp.float32)
    moe_sum = jnp.sum(
        route_gates[:, :, None] * picked.reshape(seq_count, top_count, model_width), axis=1
    )
    layer_out = (middle.astype(jnp.float32) + rms_scale(moe_sum, out_gain)).astype(jnp.bfloat16)
    return (layer_out, new_state.reshape(seq_count, head_count, HEAD_DIM * HEAD_DIM))


def solution(mesh):
    in_specs = (
        P("ep", None),
        P("ep", "tp", None),
        P(),
        P("ep", "tp"),
        P("ep", "tp"),
        P("ep", "tp"),
        P(),
        P(None, "tp"),
        P("tp"),
        P(),
        P(None, "tp"),
        P("tp"),
        P("tp"),
        P("tp"),
        P("tp", "ep"),
        P(),
        P(),
        P("ep", None),
        P("ep", None),
        P("ep", None, "tp"),
        P("ep", None, "tp"),
        P("ep", "tp", None),
        P(),
    )
    out_specs = (P("ep", None), P("ep", "tp", None))
    return jax.shard_map(local, mesh=mesh, in_specs=in_specs, out_specs=out_specs, check_vma=False)
```

profile of v0, /device:TPU:0, one launch (start us, length us, event | category | flops | bytes accessed | tf_op | source)
XLA Modules:
  0.0 255.9 jit_solution(16178982749904903208)
XLA Ops:
  7.2 0.0 copy-start
  7.3 0.0 reduce-scatter.2.cloned.1.call-start
  7.3 1.1 fusion.55
  8.4 0.9 fusion.57
  9.4 14.0 %all_to_all.29 = bf16[16,8,256]{2,0,1:T(8,128)(2,1)S(1)} all-to-all(bf16[16,8,256]{2,0,1:T(8,128)(2,1)S(1)} %bitcast.77), channel_id=1, replica_groups=mesh['ep'=8,'tp'=4] {'ep'}, dimensions={1} | all-to-all | bytes 131072 | tf_op jit(solution)/shard_map/all_to_all | solution.py:53
  23.4 2.3 fusion.39
  25.6 0.0 reduce-scatter.2.cloned.1.call-update
  25.6 0.0 all-gather.2.cloned.1.call-start
  25.7 0.7 all-gather.2.cloned.1.call-update
  26.4 0.0 all-reduce.3.cloned.1.call-start
  26.4 0.0 copy-done.14
  26.5 0.1 mul.287
  26.5 0.0 copy-done.10
  26.5 0.3 fusion.34
  26.9 0.1 reshape.217
  27.0 0.0 copy-done.5
  27.0 0.4 fusion.74
  27.4 0.1 mul.284
  27.4 4.6 %reshape.214 = f32[16,8,64,64]{3,2,1,0:T(8,128)} reshape(f32[16,8,4096]{2,1,0:T(8,128)} %param.24) | data formatting | bytes 4194304 | tf_op jit(solution)/shard_map/reshape | solution.py:83
  32.1 2.2 mul.285
  34.3 4.8 %mul.309 = f32[16,8,4096]{2,1,0:T(8,128)} reshape(f32[16,8,64,64]{3,2,1,0:T(8,128)} %mul.285) | data formatting | bytes 4194304 | tf_op jit(solution)/shard_map/mul | solution.py:86
  39.1 0.1 copy.46
  39.2 0.1 eq.58
  39.3 0.1 fusion.75
  39.3 0.1 reduce_window_sum.11
  39.4 0.2 select_reduce_fusion
  39.6 0.1 reduce_sum.121
  39.7 0.1 copy.47
  39.8 46.8 %reduce-scatter.2.cloned.1.call-done = f32[16,1536]{1,0:T(8,128)} async-done(((f32[128,1536]{1,0:T(8,128)}), f32[16,1536]{1,0:T(8,128)}) %reduce-scatter.2.cloned.1.call-update) | async-done | bytes 98320 | tf_op jit(solution)/shard_map/reduce_scatter | solution.py:55
  86.6 0.9 convert.9
  87.5 0.1 reshape.226
  87.6 0.1 reshape.228
  87.7 0.1 reshape.227
  87.8 0.1 multiply_reduce_fusion.5
  87.9 0.1 fusion.88
  88.0 20.2 %broadcast_multiply_fusion = (f32[16,8,64,64]{3,2,1,0:T(8,128)}, f32[16,8,64]{2,1,0:T(8,128)S(1)}, f32[16,8,64,64]{3,2,1,0:T(8,128)}) fusion(f32[16,8,64]{2,1,0:T(8,128)S(1)} %get-tuple-element.10, f32[16,8,64]{2,1,0:T(8,128)S(1)} %reshape.227, f32[16,8,64]{2,1,0:T(8,128)S(1)} %reshape.228, f32[16,8,64,64]{3,2,1,0:T(8,128)} %reshape.214, ...), kind=kOutput, calls=%fused_computation.17 | output fusion | flops 4194367 | bytes 6520832 | tf_op jit(solution)/shard_map/mul | solution.py:87
  108.2 4.8 %mul.311 = f32[16,8,4096]{2,1,0:T(8,128)} reshape(f32[16,8,64,64]{3,2,1,0:T(8,128)} %get-tuple-element.14) | data formatting | bytes 4194304 | tf_op jit(solution)/shard_map/mul | solution.py:87
  113.0 4.9 %mul.312 = f32[16,8,4096]{2,1,0:T(8,128)} reshape(f32[16,8,64,64]{3,2,1,0:T(8,128)} %get-tuple-element.8) | data formatting | bytes 4194304 | tf_op jit(solution)/shard_map/mul | solution.py:88
  117.9 2.2 mul.307
  120.1 4.8 %mul.313 = f32[16,8,4096]{2,1,0:T(8,128)} reshape(f32[16,8,64,64]{3,2,1,0:T(8,128)} %mul.307) | data formatting | bytes 4194304 | tf_op jit(solution)/shard_map/mul | solution.py:90
  124.9 5.9 %multiply_reduce_fusion.2 = (f32[16,8]{1,0:T(8,128)S(1)}, f32[16,8,4096]{2,1,0:T(8,128)}) fusion(f32[16,8,4096]{2,1,0:T(8,128)} %mul.313, f32[16,8,4096]{2,1,0:T(8,128)} %mul.312, f32[16,8,4096]{2,1,0:T(8,128)} %mul.311, f32[16,8,4096]{2,1,0:T(8,128)} %param.24, f32[16,8,4096]{2,1,0:T(8,128)} %mul.309), kind=kLoop, calls=%fused_computation.15 | loop fusion | flops 2621312 | bytes 12583424 | tf_op jit(solution)/shard_map/reduce_sum | solution.py:91
  130.8 0.2 multiply_reduce_fusion.4
  131.0 0.1 subtract_multiply_fusion
  131.1 0.1 mul.318
  131.2 6.9 %all-gather.2.cloned.1.call-done = bf16[512,2048]{1,0:T(8,128)(2,1)} async-done(((bf16[512,256]{1,0:T(8,128)(2,1)}), bf16[512,2048]{1,0:T(8,128)(2,1)}) %all-gather.2.cloned.1.call-update) | async-done | bytes 2097168 | tf_op jit(solution)/shard_map/all_gather | solution.py:102
  138.1 2.6 %convolution_convert_fusion.2 = bf16[16,2048]{1,0:T(8,128)(2,1)} fusion(bf16[512,2048]{1,0:T(8,128)(2,1)} %all-gather.2.cloned.1.call-done, f32[16,512]{1,0:T(8,128)S(1)} %mul.318, f32[512]{0:T(512)S(1)} %copy-done.12), kind=kOutput, calls=%fused_computation.8 | convolution fusion | flops 33603584 | bytes 2197504 | tf_op jit(solution)/shard_map/dot_general | solution.py:100
  140.7 0.0 all-reduce.3.cloned.1.call-update
  140.7 0.0 all-reduce.5.cloned.1.call-start
  140.8 0.1 fusion.79
  140.9 29.9 %all-reduce.3.cloned.1.call-done = bf16[16,2048]{1,0:T(8,128)(2,1)} async-done(((bf16[16,2048]{1,0:T(8,128)(2,1)}), bf16[16,2048]{1,0:T(8,128)(2,1)}) %all-reduce.3.cloned.1.call-update) | async-done | bytes 65552 | tf_op jit(solution)/shard_map/psum | solution.py:105
  170.8 1.0 fusion.53
  171.7 0.0 copy-done.7
  171.7 1.1 fusion.59
  172.8 0.3 convolution_convert_fusion.1
  173.2 18.7 %all_to_all.30 = bf16[8,1,16,2048]{3,2,1,0:T(8,128)(2,1)S(1)} all-to-all(bf16[8,1,16,2048]{3,2,1,0:T(8,128)(2,1)S(1)} %bitcast.74), channel_id=1, replica_groups=mesh['ep'=8,'tp'=4] {'ep'}, dimensions={0} | all-to-all | bytes 1048576 | tf_op jit(solution)/shard_map/all_to_all | solution.py:130
  191.9 2.0 fusion.16
  193.9 0.0 copy-start.13
  193.9 3.3 %fusion.2 = bf16[8,1,16,2048]{3,2,0,1:T(8,128)(2,1)} fusion(bf16[1,512,2048]{2,1,0:T(8,128)(2,1)S(1)} %copy-done, f32[8,16,512]{2,1,0:T(8,128)S(1)} %fusion.16, bf16[1,2048,512]{2,1,0:T(8,128)(2,1)} %param.43, bf16[8,1,16,2048]{3,2,1,0:T(8,128)(2,1)S(1)} %all_to_all.30), kind=kOutput, calls=%fused_computation.7 | convolution fusion | flops 537722880 | bytes 5505024 | tf_op jit(solution)/shard_map/seif,efd->seid/dot_general | solution.py:143
  197.2 0.0 all-reduce.5.cloned.1.call-update
  197.2 32.0 %all-reduce.5.cloned.1.call-done = bf16[8,1,16,2048]{3,2,0,1:T(8,128)(2,1)} async-done(((bf16[8,1,16,2048]{3,2,0,1:T(8,128)(2,1)}), bf16[8,1,16,2048]{3,2,0,1:T(8,128)(2,1)}) %all-reduce.5.cloned.1.call-update) | async-done | bytes 524304 | tf_op jit(solution)/shard_map/psum | solution.py:146
  229.2 19.0 %all_to_all.31 = bf16[8,1,16,2048]{3,2,1,0:T(8,128)(2,1)S(1)} all-to-all(bf16[8,1,16,2048]{3,2,1,0:T(8,128)(2,1)} %bitcast.76), channel_id=1, replica_groups=mesh['ep'=8,'tp'=4] {'ep'}, dimensions={0} | all-to-all | bytes 1048576 | tf_op jit(solution)/shard_map/all_to_all | solution.py:147
  248.3 0.3 fusion.12
  248.5 0.1 multiply_reduce_fusion.3
  248.7 0.7 fusion.62
  (34 shorter events, 0.1 us)
Async XLA Ops:
  7.2 186.7 %copy-start = (bf16[1,512,2048]{2,1,0:T(8,128)(2,1)S(1)}, bf16[1,512,2048]{2,1,0:T(8,128)(2,1)}, u32[]{:S(2)}) copy-start(bf16[1,512,2048]{2,1,0:T(8,128)(2,1)} %param.44) | copy-start | bytes 6291460
  7.2 19.3 %copy-start.14 = (f32[512]{0:T(512)S(1)}, f32[512]{0:T(512)}, u32[]{:S(2)}) copy-start(f32[512]{0:T(512)} %param.35) | copy-start | bytes 6148
  7.2 19.3 %copy-start.2 = (bf16[2048,64]{0,1:T(8,128)(2,1)S(1)}, bf16[2048,64]{0,1:T(8,128)(2,1)}, u32[]{:S(2)}) copy-start(bf16[2048,64]{0,1:T(8,128)(2,1)} %param.32) | copy-start | bytes 786436
  7.2 19.3 %copy-start.4 = (bf16[64,512]{1,0:T(8,128)(2,1)S(1)}, bf16[64,512]{1,0:T(8,128)(2,1)}, u32[]{:S(2)}) copy-start(bf16[64,512]{1,0:T(8,128)(2,1)} %param.33) | copy-start | bytes 196612
  7.2 19.3 %copy-start.10 = (f32[512]{0:T(512)S(1)}, f32[512]{0:T(512)}, u32[]{:S(2)}) copy-start(f32[512]{0:T(512)} %param.34) | copy-start | bytes 6148
  7.2 19.7 %copy-start.3 = (bf16[2048,64]{0,1:T(8,128)(2,1)S(1)}, bf16[2048,64]{0,1:T(8,128)(2,1)}, u32[]{:S(2)}) copy-start(bf16[2048,64]{0,1:T(8,128)(2,1)} %param.29) | copy-start | bytes 786436
  7.2 19.7 %copy-start.5 = (bf16[64,512]{1,0:T(8,128)(2,1)S(1)}, bf16[64,512]{1,0:T(8,128)(2,1)}, u32[]{:S(2)}) copy-start(bf16[64,512]{1,0:T(8,128)(2,1)} %param.30) | copy-start | bytes 196612
  7.2 19.7 %copy-start.11 = (f32[512]{0:T(512)S(1)}, f32[512]{0:T(512)}, u32[]{:S(2)}) copy-start(f32[512]{0:T(512)} %param.31) | copy-start | bytes 6148
  7.3 79.4 %reduce-scatter.2.cloned.1.call-start = ((), (), s32[]{:S(2)}) async-start(), calls=%async_computation.4 | async-start | bytes 884736 | tf_op jit(solution)/shard_map/reduce_scatter | solution.py:55
  25.6 112.4 %all-gather.2.cloned.1.call-start = ((), (), s32[]{:S(2)}) async-start(), calls=%async_computation.5 | async-start | bytes 2359296 | tf_op jit(solution)/shard_map/all_gather | solution.py:102
  26.4 144.4 %all-reduce.3.cloned.1.call-start = ((), (), s32[]{:S(2)}) async-start(), calls=%async_computation.6 | async-start | bytes 131072 | tf_op jit(solution)/shard_map/psum | solution.py:105
  34.3 4.8 %copy-start.9 = (s32[16,4]{0,1:T(4,128)S(1)}, s32[16,4]{0,1:T(4,128)}, u32[]{:S(2)}) copy-start(s32[16,4]{0,1:T(4,128)} %param.40) | copy-start | bytes 772
  124.9 13.2 %copy-start.12 = (f32[512]{0:T(512)S(1)}, f32[512]{0:T(512)}, u32[]{:S(2)}) copy-start(f32[512]{0:T(512)} %param.36) | copy-start | bytes 6148
  130.8 40.9 %copy-start.1 = (bf16[16,2048]{1,0:T(8,128)(2,1)S(1)}, bf16[16,2048]{1,0:T(8,128)(2,1)}, u32[]{:S(2)}) copy-start(bf16[16,2048]{1,0:T(8,128)(2,1)} %param.23) | copy-start | bytes 196612
  130.8 40.9 %copy-start.7 = (f32[2048]{0:T(1024)S(1)}, f32[2048]{0:T(1024)}, u32[]{:S(2)}) copy-start(f32[2048]{0:T(1024)} %param.38) | copy-start | bytes 24580
  130.8 42.0 %copy-start.6 = (f32[2048]{0:T(1024)S(1)}, f32[2048]{0:T(1024)}, u32[]{:S(2)}) copy-start(f32[2048]{0:T(1024)} %param.39) | copy-start | bytes 24580
  140.7 88.5 %all-reduce.5.cloned.1.call-start = ((), (), s32[]{:S(2)}) async-start(), calls=%async_computation.7 | async-start | bytes 1048576 | tf_op jit(solution)/shard_map/psum | solution.py:146
  193.9 54.3 %copy-start.13 = (f32[16,4]{0,1:T(4,128)S(1)}, f32[16,4]{0,1:T(4,128)}, u32[]{:S(2)}) copy-start(f32[16,4]{0,1:T(4,128)} %param.41) | copy-start | bytes 772
  197.2 51.5 %copy-start.8 = (f32[2048]{0:T(1024)S(1)}, f32[2048]{0:T(1024)}, u32[]{:S(2)}) copy-start(f32[2048]{0:T(1024)} %param.45) | copy-start | bytes 24580
Sparse Core Ops, SparseCore 0:
  25.8 60.8 reduce-scatter.1
  88.7 49.3 all-gather.1
  141.0 29.7 all-reduce.2
  197.3 31.8 all-reduce.4
where the time goes:
time: 257 us; the launch traced here: 256 us
  waiting for transfers between devices  116 us (45%)
  blocking collectives  51.7 us (20%)
  other arithmetic  32.8 us (13%)
  local copies, waits for them, and re-layouts  29.3 us (11%)
  between operations  14 us (5%)
  matrix products  11.5 us (4%)
    reduce_scatter x1, waiting for transfers between devices, local(): lax.psum_scatter(jnp.dot(spread_rows, joined, preferred_element_type=jnp....  46.8 us
    psum x1, waiting for transfers between devices, local(): returned = lax.psum(partial_value.astype(jnp.bfloat16), 'tp')  32 us
    psum x1, waiting for transfers between devices, local(): lax.psum(head_partial.astype(jnp.bfloat16), 'tp').astype(jnp.float32)  29.9 us
    mul x1, other arithmetic, local(): along_key[..., None] * (unit_key * learn_rate)[:, :, None, :]  20.2 us
    all_to_all x1, blocking collectives, local(): lax.all_to_all(returned, 'ep', split_axis=0, concat_axis=0, tiled=True)  19 us
    all_to_all x1, blocking collectives, local(): lax.all_to_all(send_rows, 'ep', split_axis=0, concat_axis=0, tiled=True)  18.7 us
    all_to_all x1, blocking collectives, local(): lax.all_to_all(normed_in, 'ep', split_axis=1, concat_axis=0, tiled=True)  14 us
    mul x3, local copies, waits for them, and re-layouts, local(): readout = jnp.sum(new_state * rec_rows[:, :, None, :], axis=-1)  7.12 us
  transfers between devices with their start and end apart: 4, of which 4 were waited for; matrix products, arithmetic and copies ran while one was open for 23% of the time, Pallas kernels for 0%

commit v1 on v0

--- a/solution.py
+++ b/solution.py
@@ -1,9 +1,15 @@
+import functools
+import math
+
 import jax
 import jax.numpy as jnp
 from jax import lax
+from jax.experimental import pallas as pl
+from jax.experimental.pallas import tpu as pltpu
 from jax.sharding import PartitionSpec as P
 
 HEAD_DIM = 64
+MESH = pl.DeviceIdType.MESH
 
 
 norm_eps = 1e-06
@@ -155,6 +161,457 @@
     return (layer_out, new_state.reshape(seq_count, head_count, HEAD_DIM * HEAD_DIM))
 
 
+def power_of_two(value):
+    return value > 0 and value & (value - 1) == 0
+
+
+def row_scale(values):
+    return values * lax.rsqrt(jnp.mean(values * values, axis=-1, keepdims=True) + norm_eps)
+
+
+def layer_kernel(
+    n,
+    m,
+    layer_in,
+    mix_gain,
+    decay_base,
+    rate_base,
+    key_scale,
+    group_gain,
+    post_gain,
+    ffn_gain,
+    out_gain,
+    routes,
+    route_gates,
+    state_hbm,
+    rec_hbm,
+    key_hbm,
+    val_hbm,
+    ddown_hbm,
+    dup_hbm,
+    rdown_hbm,
+    rup_hbm,
+    out_hbm,
+    egate_hbm,
+    eup_hbm,
+    edown_hbm,
+    layer_out,
+    new_state,
+    state_v,
+    proj_v,
+    ddown_v,
+    dup_v,
+    rdown_v,
+    rup_v,
+    out_v,
+    egate_v,
+    eup_v,
+    edown_v,
+    spread_v,
+    gather_t,
+    products,
+    fresh_v,
+    s1,
+    r1,
+    s2,
+    r2,
+    a3,
+    s4,
+    p5,
+    f6,
+    a6,
+    s7,
+    r7,
+    s8,
+    r8,
+    a9,
+    local_sem,
+    ep_send,
+    ep_recv,
+    tp_send,
+    tp_recv,
+    fw_send,
+    fw_recv,
+):
+    e = lax.axis_index("ep")
+    t = lax.axis_index("tp")
+    seqs, width = layer_in.shape
+    heads = state_hbm.shape[1]
+    flat = state_hbm.shape[2]
+    cols = rec_hbm.shape[1]
+    rows = rec_hbm.shape[0]
+    pairs = seqs * heads
+    tokens = n * seqs
+    f32 = jnp.float32
+    bf16 = jnp.bfloat16
+
+    loads = [
+        pltpu.make_async_copy(source, target, local_sem.at[i])
+        for i, (source, target) in enumerate(
+            (
+                (ddown_hbm, ddown_v),
+                (rdown_hbm, rdown_v),
+                (dup_hbm, dup_v),
+                (rup_hbm, rup_v),
+                (rec_hbm, proj_v.at[0]),
+                (key_hbm, proj_v.at[1]),
+                (val_hbm, proj_v.at[2]),
+                (state_hbm, state_v),
+                (out_hbm, out_v),
+                (egate_hbm.at[0], egate_v),
+                (eup_hbm.at[0], eup_v),
+                (edown_hbm.at[0], edown_v),
+            )
+        )
+    ]
+    barrier = pltpu.get_barrier_semaphore()
+    for d in range(1, n):
+        pl.semaphore_signal(barrier, inc=1, device_id=(lax.rem(e + d, n), t), device_id_type=MESH)
+    for d in range(1, m):
+        pl.semaphore_signal(barrier, inc=1, device_id=(e, lax.rem(t + d, m)), device_id_type=MESH)
+    for load in loads:
+        load.start()
+
+    def ep_copy(phase, d, source, target):
+        return pltpu.make_async_remote_copy(
+            src_ref=source,
+            dst_ref=target,
+            send_sem=ep_send.at[phase, d],
+            recv_sem=ep_recv.at[phase, d],
+            device_id=(lax.rem(e + d, n), t),
+            device_id_type=MESH,
+        )
+
+    def tp_copy(phase, d, source, target):
+        return pltpu.make_async_remote_copy(
+            src_ref=source,
+            dst_ref=target,
+            send_sem=tp_send.at[phase, d],
+            recv_sem=tp_recv.at[phase, d],
+            device_id=(e, lax.rem(t + d, m)),
+            device_id_type=MESH,
+        )
+
+    sent = []
+
+    def start(copies):
+        for copy in copies:
+            copy.start()
+        sent.extend(copies)
+        return copies
+
+    token_in = layer_in[...].astype(f32)
+    normed = (row_scale(token_in) * mix_gain[...]).astype(bf16)
+    for j in range(n):
+        s1[j] = normed[:, j * rows : (j + 1) * rows]
+    r1[e] = s1[e]
+    pl.semaphore_wait(barrier, n - 1 + m - 1)
+    first = start([ep_copy(0, d, s1.at[lax.rem(e + d, n)], r1.at[e]) for d in range(1, n)])
+
+    for load in loads[:4]:
+        load.wait()
+    decay_hidden = jnp.tanh(jnp.dot(normed, ddown_v[...], preferred_element_type=f32)).astype(bf16)
+    rate_hidden = jnp.dot(normed, rdown_v[...], preferred_element_type=f32).astype(bf16)
+    decay_pre = decay_base[...] + jnp.dot(decay_hidden, dup_v[...], preferred_element_type=f32)
+    rate_pre = rate_base[...] + jnp.dot(rate_hidden, rup_v[...], preferred_element_type=f32)
+    scale_wide = jnp.broadcast_to(key_scale[...], (seqs, cols))
+
+    def head_major(values):
+        return jnp.concatenate(
+            [values[:, h * HEAD_DIM : (h + 1) * HEAD_DIM] for h in range(heads)], axis=0
+        )
+
+    head_bits = int(math.log2(heads))
+    seq_bits = int(math.log2(seqs))
+    dim_bits = int(math.log2(HEAD_DIM))
+    i0 = lax.broadcasted_iota(jnp.int32, (pairs, pairs), 0)
+    i1 = lax.broadcasted_iota(jnp.int32, (pairs, pairs), 1)
+    to_pairs = (i1 == ((i0 & (heads - 1)) << seq_bits) + (i0 >> head_bits)).astype(f32)
+    from_pairs = (i0 == ((i1 & (heads - 1)) << seq_bits) + (i1 >> head_bits)).astype(bf16)
+
+    side = jnp.concatenate(
+        [head_major(decay_pre), head_major(rate_pre), head_major(scale_wide)], axis=1
+    )
+    side = jnp.dot(to_pairs, side, preferred_element_type=f32, precision=lax.Precision.HIGHEST)
+    decay = jnp.exp(jax.nn.sigmoid(side[:, :HEAD_DIM]) * -math.exp(-0.5))
+    rate = jax.nn.sigmoid(side[:, HEAD_DIM : 2 * HEAD_DIM])
+    scale = side[:, 2 * HEAD_DIM :]
+    c0 = lax.broadcasted_iota(jnp.int32, (2 * HEAD_DIM, flat), 0) & (HEAD_DIM - 1)
+    c1 = lax.broadcasted_iota(jnp.int32, (2 * HEAD_DIM, flat), 1) >> dim_bits
+    spread_v[...] = (c0 == c1).astype(f32).astype(bf16)
+    g0 = lax.broadcasted_iota(jnp.int32, (flat, HEAD_DIM), 0) >> dim_bits
+    g1 = lax.broadcasted_iota(jnp.int32, (flat, HEAD_DIM), 1)
+    gather_t[...] = (g0 == g1).astype(f32).astype(bf16)
+
+    for load in loads[4:7]:
+        load.wait()
+    for copy in first:
+        copy.wait_recv()
+    spread_rows = r1[...].reshape(tokens, rows)
+    for w in range(3):
+        part = jnp.dot(spread_rows, proj_v[w], preferred_element_type=f32).astype(bf16)
+        s2[:, :, w * cols : (w + 1) * cols] = part.reshape(n, seqs, cols)
+    r2[e] = s2[e]
+    second = start([ep_copy(1, d, s2.at[lax.rem(e + d, n)], r2.at[e]) for d in range(1, n)])
+    loads[7].wait()
+    for copy in second:
+        copy.wait_recv()
+    total = r2[0].astype(f32)
+    for j in range(1, n):
+        total = total + r2[j].astype(f32)
+    total = total.astype(bf16).astype(f32)
+    heads_in = jnp.concatenate(
+        [head_major(total[:, w * cols : (w + 1) * cols]) for w in range(3)], axis=1
+    ).astype(bf16)
+    heads_in = jnp.dot(to_pairs.astype(bf16), heads_in, preferred_element_type=f32)
+    rec = heads_in[:, :HEAD_DIM]
+    key = heads_in[:, HEAD_DIM : 2 * HEAD_DIM]
+    val = heads_in[:, 2 * HEAD_DIM :]
+    scaled = key * scale
+    unit = scaled * lax.rsqrt(jnp.sum(scaled * scaled, axis=-1, keepdims=True) + norm_eps)
+    unit_rate = unit * rate
+    key_rate = key * rate
+    decay_rec = decay * rec
+    along_gain = jnp.sum(unit_rate * rec, axis=-1, keepdims=True)
+    val_gain = jnp.sum(key_rate * rec, axis=-1, keepdims=True)
+
+    lanes = 2 * HEAD_DIM
+    two = lambda values: jnp.concatenate([values, values], axis=1)
+    unit2, decay_rec2 = two(unit), two(decay_rec)
+
+    def products_step(j, carry):
+        at = pl.ds(pl.multiple_of(j * lanes, lanes), lanes)
+        block = state_v[:, :, at].reshape(pairs, lanes)
+        for i, factor in enumerate((unit2, decay_rec2)):
+            value = block * factor
+            high = value.astype(bf16)
+            products[2 * i * pairs : (2 * i + 1) * pairs, at] = high
+            products[(2 * i + 1) * pairs : (2 * i + 2) * pairs, at] = (
+                value - high.astype(f32)
+            ).astype(bf16)
+        return carry
+
+    lax.fori_loop(0, flat // lanes, products_step, 0)
+    reduced = jnp.dot(products[...], gather_t[...], preferred_element_type=f32)
+    along = reduced[:pairs] + reduced[pairs : 2 * pairs]
+    readout = (
+        reduced[2 * pairs : 3 * pairs] + reduced[3 * pairs :] - along * along_gain + val * val_gain
+    )
+    centred = readout - jnp.mean(readout, axis=-1, keepdims=True)
+    normed_out = centred * lax.rsqrt(jnp.mean(centred * centred, axis=-1, keepdims=True) + group_eps)
+    out_high = normed_out.astype(bf16)
+    out_low = (normed_out - out_high.astype(f32)).astype(bf16)
+    back = jnp.dot(
+        from_pairs, jnp.concatenate([out_high, out_low], axis=1), preferred_element_type=f32
+    )
+    back = back[:, :HEAD_DIM] + back[:, HEAD_DIM:]
+    back = jnp.concatenate([back[h * seqs : (h + 1) * seqs] for h in range(heads)], axis=1)
+    a3[e] = (back * group_gain[...]).astype(bf16)
+    third = start([ep_copy(2, d, a3.at[e], a3.at[e]) for d in range(1, n)])
+
+    along_high = along.astype(bf16)
+    along_low = (along - along_high.astype(f32)).astype(bf16)
+    along_pair = jnp.concatenate([along_high, along_low], axis=1)
+    val_low = val.astype(bf16)
+    decay2, unit_rate2, key_rate2 = two(decay), two(unit_rate), two(key_rate)
+
+    def fresh_step(j, carry):
+        at = pl.ds(pl.multiple_of(j * lanes, lanes), lanes)
+        block = state_v[:, :, at].reshape(pairs, lanes)
+        table = spread_v[:, at]
+        along_wide = jnp.dot(along_pair, table, preferred_element_type=f32)
+        val_wide = jnp.dot(val_low, table[:HEAD_DIM], preferred_element_type=f32)
+        fresh = block * decay2 - along_wide * unit_rate2 + val_wide * key_rate2
+        fresh_v[:, :, at] = fresh.reshape(seqs, heads, lanes)
+        return carry
+
+    lax.fori_loop(0, flat // lanes, fresh_step, 0)
+    store = pltpu.make_async_copy(fresh_v, new_state, local_sem.at[len(loads)])
+    store.start()
+
+    loads[8].wait()
+    for copy in third:
+        copy.wait_recv()
+    part = jnp.dot(a3[...].reshape(tokens, cols), out_v[...], preferred_element_type=f32)
+    s4[...] = part.astype(bf16).reshape(n, seqs, rows)
+    p5[t, e] = s4[e]
+    fourth = start([ep_copy(3, d, s4.at[lax.rem(e + d, n)], p5.at[t, e]) for d in range(1, n)])
+    for copy in fourth:
+        copy.wait_recv()
+    fifth = start([tp_copy(0, d, p5.at[t], p5.at[t]) for d in range(1, m)])
+    for copy in fifth:
+        copy.wait_recv()
+    mixed = p5[0].astype(f32)
+    for q in range(1, m):
+        mixed = mixed + p5[q].astype(f32)
+    mixed = jnp.concatenate([mixed[j] for j in range(n)], axis=1)
+    middle = (token_in + row_scale(mixed) * post_gain[...]).astype(bf16).astype(f32)
+    ffn_in = (row_scale(middle) * ffn_gain[...]).astype(bf16)
+
+    for q in range(m):
+        f6[q] = ffn_in[:, q * cols : (q + 1) * cols]
+        a6[q, e] = ffn_in[:, q * cols : (q + 1) * cols]
+    sixth = start([ep_copy(4, d, f6.at[t], a6.at[t, e]) for d in range(1, n)])
+    passed = {}
+    for d in range(1, n):
+        sixth[d - 1].wait_recv()
+        source = lax.rem(e + n - d, n)
+        for k in range(1, m):
+            passed[d, k] = pltpu.make_async_remote_copy(
+                src_ref=a6.at[t, source],
+                dst_ref=a6.at[t, source],
+                send_sem=fw_send.at[d, k],
+                recv_sem=fw_recv.at[d, k],
+                device_id=(e, lax.rem(t + k, m)),
+                device_id_type=MESH,
+            )
+            start([passed[d, k]])
+    for load in loads[9:]:
+        load.wait()
+    gate = jnp.zeros((tokens, egate_hbm.shape[2]), f32)
+    up = gate
+    for k in range(m):
+        q = lax.rem(t + m - k, m)
+        if k > 0:
+            for d in range(1, n):
+                passed[d, k].wait_recv()
+        taken = a6[q].reshape(tokens, cols)
+        at = pl.ds(pl.multiple_of(q * cols, cols), cols)
+        gate = gate + jnp.dot(taken, egate_v[at, :], preferred_element_type=f32)
+        up = up + jnp.dot(taken, eup_v[at, :], preferred_element_type=f32)
+    gate = jnp.minimum(gate, clamp_limit)
+    up = jnp.clip(up, -clamp_limit, clamp_limit)
+    hidden = ((up + 1.0) * gate * jax.nn.sigmoid(gate_alpha * gate)).astype(bf16)
+
+    seventh = []
+    for k in [2, 3, 1, 0] if m == 4 else list(range(1, m)) + [0]:
+        q = lax.rem(t + k, m)
+        at = pl.ds(pl.multiple_of(q * cols, cols), cols)
+        part = jnp.dot(hidden, edown_v[:, at], preferred_element_type=f32).astype(bf16)
+        if k == 0:
+            own = part.astype(f32)
+        else:
+            s7[q] = part
+            seventh += start([tp_copy(1, k, s7.at[q], r7.at[t])])
+    for copy in seventh:
+        copy.wait_recv()
+    for k in range(1, m):
+        own = own + r7[lax.rem(t + k, m)].astype(f32)
+    s8[...] = own.astype(bf16).reshape(n, seqs, cols)
+    r8[e] = s8[e]
+    eighth = start([ep_copy(5, d, s8.at[lax.rem(e + d, n)], r8.at[e]) for d in range(1, n)])
+    named = routes[...]
+    gates = route_gates[...]
+    for copy in eighth:
+        copy.wait_recv()
+    moe = jnp.zeros((seqs, cols), f32)
+    for j in range(n):
+        weight = jnp.sum(jnp.where(named == j, gates, 0.0), axis=1, keepdims=True)
+        moe = moe + weight * r8[j].astype(f32)
+    a9[t] = moe
+    ninth = start([tp_copy(2, d, a9.at[t], a9.at[t]) for d in range(1, m)])
+    for copy in ninth:
+        copy.wait_recv()
+    moe = jnp.concatenate([a9[q] for q in range(m)], axis=1)
+    layer_out[...] = (middle + row_scale(moe) * out_gain[...]).astype(bf16)
+    for copy in sent:
+        copy.wait_send()
+    store.wait()
+
+
+def fused_local(n, m, *args):
+    (
+        layer_in, state_in, mix_gain, rec_weight, key_weight, val_weight, decay_down, decay_up,
+        decay_base, rate_down, rate_up, rate_base, key_scale, group_gain, out_weight, post_gain,
+        ffn_gain, routes, route_gates, expert_gate, expert_up, expert_down, out_gain,
+    ) = args
+    seqs, width = layer_in.shape
+    heads, flat = state_in.shape[1:]
+    rows, cols = rec_weight.shape
+    low = decay_down.shape[1]
+    hidden = expert_gate.shape[2]
+    pairs = seqs * heads
+    tokens = n * seqs
+    f32, bf16 = jnp.float32, jnp.bfloat16
+    line = lambda values: values.reshape(1, -1)
+    vmem = pl.BlockSpec(memory_space=pltpu.VMEM)
+    hbm = pl.BlockSpec(memory_space=pl.ANY)
+    dma = pltpu.SemaphoreType.DMA
+    return pl.pallas_call(
+        functools.partial(layer_kernel, n, m),
+        out_shape=(
+            jax.ShapeDtypeStruct(layer_in.shape, bf16),
+            jax.ShapeDtypeStruct(state_in.shape, f32),
+        ),
+        in_specs=[vmem] * 11 + [hbm] * 12,
+        out_specs=(vmem, hbm),
+        scratch_shapes=[
+            pltpu.VMEM(state_in.shape, f32),
+            pltpu.VMEM((3, rows, cols), bf16),
+            pltpu.VMEM((width, low), bf16),
+            pltpu.VMEM((low, cols), bf16),
+            pltpu.VMEM((width, low), bf16),
+            pltpu.VMEM((low, cols), bf16),
+            pltpu.VMEM(out_weight.shape, bf16),
+            pltpu.VMEM((width, hidden), bf16),
+            pltpu.VMEM((width, hidden), bf16),
+            pltpu.VMEM((hidden, width), bf16),
+            pltpu.VMEM((2 * HEAD_DIM, flat), bf16),
+            pltpu.VMEM((flat, HEAD_DIM), bf16),
+            pltpu.VMEM((4 * pairs, flat), bf16),
+            pltpu.VMEM(state_in.shape, f32),
+            pltpu.VMEM((n, seqs, rows), bf16),
+            pltpu.VMEM((n, seqs, rows), bf16),
+            pltpu.VMEM((n, seqs, 3 * cols), bf16),
+            pltpu.VMEM((n, seqs, 3 * cols), bf16),
+            pltpu.VMEM((n, seqs, cols), bf16),
+            pltpu.VMEM((n, seqs, rows), bf16),
+            pltpu.VMEM((m, n, seqs, rows), bf16),
+            pltpu.VMEM((m, seqs, cols), bf16),
+            pltpu.VMEM((m, n, seqs, cols), bf16),
+            pltpu.VMEM((m, tokens, cols), bf16),
+            pltpu.VMEM((m, tokens, cols), bf16),
+            pltpu.VMEM((n, seqs, cols), bf16),
+            pltpu.VMEM((n, seqs, cols), bf16),
+            pltpu.VMEM((m, seqs, cols), f32),
+            dma((13,)),
+            dma((6, n)),
+            dma((6, n)),
+            dma((3, m)),
+            dma((3, m)),
+            dma((n, m)),
+            dma((n, m)),
+        ],
+        compiler_params=pltpu.CompilerParams(
+            collective_id=0, has_side_effects=True, vmem_limit_bytes=60 * 1024 * 1024
+        ),
+    )(
+        layer_in, line(mix_gain), line(decay_base), line(rate_base), line(key_scale),
+        line(group_gain), line(post_gain), line(ffn_gain), line(out_gain), routes, route_gates,
+        state_in, rec_weight, key_weight, val_weight, decay_down, decay_up, rate_down, rate_up,
+        out_weight, expert_gate, expert_up, expert_down,
+    )
+
+
+def choose(n, m, *args):
+    seqs, width = args[0].shape
+    heads = args[1].shape[1]
+    cols = args[3].shape[1]
+    experts = args[19].shape[0]
+    capacity = max(2, 2 * seqs * args[17].shape[1] // (n * experts))
+    if (
+        capacity >= seqs
+        and experts == 1
+        and power_of_two(seqs)
+        and power_of_two(heads)
+        and seqs % 16 == 0
+        and heads % 8 == 0
+        and cols * m == width
+    ):
+        return fused_local(n, m, *args)
+    return local(*args)
+
+
 def solution(mesh):
     in_specs = (
         P("ep", None),
@@ -182,4 +639,5 @@
         P(),
     )
     out_specs = (P("ep", None), P("ep", "tp", None))
-    return jax.shard_map(local, mesh=mesh, in_specs=in_specs, out_specs=out_specs, check_vma=False)
+    return jax.shard_map(
+        functools.partial(choose, mesh.shape["ep"], mesh.shape["tp"]), mesh=mesh, in_specs=in_specs, out_specs=out_specs, check_vma=False)

time: 257 us -> 76.8 us (0.30)
  waiting for transfers between devices: 116 us -> 0 us
  Pallas kernels: 0 us -> 64.6 us
  blocking collectives: 51.7 us -> 0 us
  other arithmetic: 32.8 us -> 0 us
  local copies, waits for them, and re-layouts: 29.3 us -> 11.2 us
  between operations: 14 us -> 0.64 us
  matrix products: 11.5 us -> 0 us
    pallas_call x0 -> x1, Pallas kernels: none -> 64.6 us  [fused_local(): pl.pallas_call(functools.partial(layer_kernel, n, m), out_shape=(jax.Shap...]
    psum x2 -> x0, waiting for transfers between devices: 61.9 us -> none  [the longest x1 32 us: local(): returned = lax.psum(partial_value.astype(jnp.bfloat16), 'tp')]
    all_to_all x3 -> x0, blocking collectives: 51.7 us -> none  [the longest x1 19 us: local(): lax.all_to_all(returned, 'ep', split_axis=0, concat_axis=0, tiled=True)]
    reduce_scatter x1 -> x0, waiting for transfers between devices: 46.8 us -> none  [local(): lax.psum_scatter(jnp.dot(spread_rows, joined, preferred_element_type=jnp....]
    mul x11 -> x0, local copies, waits for them, and re-layouts: 24.1 us -> none  [the longest x3 7.12 us: local(): readout = jnp.sum(new_state * rec_rows[:, :, None, :], axis=-1)]
    mul x3 -> x0, other arithmetic: 20.4 us -> none  [the longest x1 20.2 us: local(): along_key[..., None] * (unit_key * learn_rate)[:, :, None, :]]
    dot_general x8 -> x0, matrix products: 11.5 us -> none  [the longest x1 3.27 us: local(): jnp.einsum('seif,efd->seid', hidden, expert_down, preferred_element_type=...]
    unnamed x31 -> x6, local copies, waits for them, and re-layouts: 0.15 us -> 11.2 us
  transfers between devices with their start and end apart: 4 -> 0, of which waited for: 4 -> 0; matrix products, arithmetic and copies ran while one was open for 23% -> 0% of each run, Pallas kernels for 0% -> 0%
where the time goes in v1:
time: 76.8 us; the launch traced here: 76.4 us
  Pallas kernels  64.6 us (84%)
  local copies, waits for them, and re-layouts  11.2 us (15%)
    pallas_call x1, Pallas kernels, fused_local(): pl.pallas_call(functools.partial(layer_kernel, n, m), out_shape=(jax.Shap...  64.6 us
    unnamed x6, local copies, waits for them, and re-layouts  11.2 us

profile of v1, /device:TPU:0, one launch (start us, length us, event | category | flops | bytes accessed | tf_op | source)
XLA Modules:
  0.0 76.4 jit_solution(4653654190561202465)
XLA Ops:
  0.6 1.4 %copy.25.routes = s32[16,4]{1,0:T(8,128)} copy(s32[16,4]{0,1:T(4,128)} %param.40) | data formatting | bytes 512 | tf_op args[17]
  2.0 1.4 %copy.26.route_gates = f32[16,4]{1,0:T(8,128)} copy(f32[16,4]{0,1:T(4,128)} %param.41) | data formatting | bytes 512 | tf_op args[18]
  3.3 2.0 %copy.27.ddown_hbm = bf16[2048,64]{1,0:T(8,128)(2,1)} copy(bf16[2048,64]{0,1:T(8,128)(2,1)} %param.29) | data formatting | bytes 524288 | tf_op args[6]
  5.3 2.0 %copy.28.rdown_hbm = bf16[2048,64]{1,0:T(8,128)(2,1)} copy(bf16[2048,64]{0,1:T(8,128)(2,1)} %param.32) | data formatting | bytes 524288 | tf_op args[9]
  7.2 64.6 %shard_map.230 = (bf16[16,2048]{1,0:T(8,128)(2,1)}, f32[16,8,4096]{2,1,0:T(8,128)}) custom-call(bf16[16,2048]{1,0:T(8,128)(2,1)} %layer_in.1, f32[1,2048]{1,0:T(1,128)} %bitcast.8, f32[1,512]{1,0:T(1,128)} %bitcast.12, f32[1,512]{1,0:T(1,128)} %bitcast.13, f32[1,512]{1,0:T(1,128)} %bitcast.14, f32[1,512]{1,0:T(1,128)} %bitcast.15, f32[1,2048]{1,0:T(1,128)} %bitcast.9, ...), custom_call_target="tpu_custom_call" | custom-call | tf_op jit(solution)/shard_map/pallas_call | solution.py:540
  71.9 1.5 %copy.31 = bf16[16,2048]{1,0:T(8,128)(2,1)} copy(bf16[16,2048]{1,0:T(8,128)(2,1)} %get-tuple-element.4) | data formatting | bytes 131072
  73.3 3.1 %copy.32 = f32[16,8,4096]{2,1,0:T(8,128)} copy(f32[16,8,4096]{2,1,0:T(8,128)} %get-tuple-element.5) | data formatting | bytes 4194304

commit v2 on v1

--- a/solution.py
+++ b/solution.py
@@ -245,6 +245,9 @@
     f32 = jnp.float32
     bf16 = jnp.bfloat16
 
+    def across(left, right):
+        return lax.dot_general(left, right, (((1,), (1,)), ((), ())), preferred_element_type=f32)
+
     loads = [
         pltpu.make_async_copy(source, target, local_sem.at[i])
         for i, (source, target) in enumerate(
@@ -310,8 +313,8 @@
 
     for load in loads[:4]:
         load.wait()
-    decay_hidden = jnp.tanh(jnp.dot(normed, ddown_v[...], preferred_element_type=f32)).astype(bf16)
-    rate_hidden = jnp.dot(normed, rdown_v[...], preferred_element_type=f32).astype(bf16)
+    decay_hidden = jnp.tanh(across(normed, ddown_v[...])).astype(bf16)
+    rate_hidden = across(normed, rdown_v[...]).astype(bf16)
     decay_pre = decay_base[...] + jnp.dot(decay_hidden, dup_v[...], preferred_element_type=f32)
     rate_pre = rate_base[...] + jnp.dot(rate_hidden, rup_v[...], preferred_element_type=f32)
     scale_wide = jnp.broadcast_to(key_scale[...], (seqs, cols))
@@ -380,18 +383,19 @@
     unit2, decay_rec2 = two(unit), two(decay_rec)
 
     def products_step(j, carry):
-        at = pl.ds(pl.multiple_of(j * lanes, lanes), lanes)
-        block = state_v[:, :, at].reshape(pairs, lanes)
-        for i, factor in enumerate((unit2, decay_rec2)):
-            value = block * factor
-            high = value.astype(bf16)
-            products[2 * i * pairs : (2 * i + 1) * pairs, at] = high
-            products[(2 * i + 1) * pairs : (2 * i + 2) * pairs, at] = (
-                value - high.astype(f32)
-            ).astype(bf16)
+        for piece in range(4):
+            at = pl.ds(pl.multiple_of((4 * j + piece) * lanes, lanes), lanes)
+            block = state_v[:, :, at].reshape(pairs, lanes)
+            for i, factor in enumerate((unit2, decay_rec2)):
+                value = block * factor
+                high = value.astype(bf16)
+                products[2 * i * pairs : (2 * i + 1) * pairs, at] = high
+                products[(2 * i + 1) * pairs : (2 * i + 2) * pairs, at] = (
+                    value - high.astype(f32)
+                ).astype(bf16)
         return carry
 
-    lax.fori_loop(0, flat // lanes, products_step, 0)
+    lax.fori_loop(0, flat // lanes // 4, products_step, 0)
     reduced = jnp.dot(products[...], gather_t[...], preferred_element_type=f32)
     along = reduced[:pairs] + reduced[pairs : 2 * pairs]
     readout = (
@@ -416,16 +420,21 @@
     decay2, unit_rate2, key_rate2 = two(decay), two(unit_rate), two(key_rate)
 
     def fresh_step(j, carry):
-        at = pl.ds(pl.multiple_of(j * lanes, lanes), lanes)
-        block = state_v[:, :, at].reshape(pairs, lanes)
-        table = spread_v[:, at]
+        whole = pl.ds(pl.multiple_of(4 * j * lanes, 4 * lanes), 4 * lanes)
+        table = spread_v[:, whole]
         along_wide = jnp.dot(along_pair, table, preferred_element_type=f32)
         val_wide = jnp.dot(val_low, table[:HEAD_DIM], preferred_element_type=f32)
-        fresh = block * decay2 - along_wide * unit_rate2 + val_wide * key_rate2
-        fresh_v[:, :, at] = fresh.reshape(seqs, heads, lanes)
+        for piece in range(4):
+            at = pl.ds(pl.multiple_of((4 * j + piece) * lanes, lanes), lanes)
+            block = state_v[:, :, at].reshape(pairs, lanes)
+            cut = slice(piece * lanes, (piece + 1) * lanes)
+            fresh = (
+                block * decay2 - along_wide[:, cut] * unit_rate2 + val_wide[:, cut] * key_rate2
+            )
+            fresh_v[:, :, at] = fresh.reshape(seqs, heads, lanes)
         return carry
 
-    lax.fori_loop(0, flat // lanes, fresh_step, 0)
+    lax.fori_loop(0, flat // lanes // 4, fresh_step, 0)
     store = pltpu.make_async_copy(fresh_v, new_state, local_sem.at[len(loads)])
     store.start()
 
@@ -452,67 +461,104 @@
         f6[q] = ffn_in[:, q * cols : (q + 1) * cols]
         a6[q, e] = ffn_in[:, q * cols : (q + 1) * cols]
     sixth = start([ep_copy(4, d, f6.at[t], a6.at[t, e]) for d in range(1, n)])
-    passed = {}
+    near = t + 1 - 2 * lax.rem(t, 2)
+    far = lax.rem(t + 2, m)
+    cross = lax.rem(near + 2, m)
+
+    def pass_on(kind, d, quarter, target):
+        source = lax.rem(e + n - d, n)
+        copy = pltpu.make_async_remote_copy(
+            src_ref=a6.at[quarter, source],
+            dst_ref=a6.at[quarter, source],
+            send_sem=fw_send.at[d, kind],
+            recv_sem=fw_recv.at[d, kind],
+            device_id=(e, target),
+            device_id_type=MESH,
+        )
+        return start([copy])[0]
+
+    to_far, to_near, relayed = [], [], []
     for d in range(1, n):
         sixth[d - 1].wait_recv()
-        source = lax.rem(e + n - d, n)
-        for k in range(1, m):
-            passed[d, k] = pltpu.make_async_remote_copy(
-                src_ref=a6.at[t, source],
-                dst_ref=a6.at[t, source],
-                send_sem=fw_send.at[d, k],
-                recv_sem=fw_recv.at[d, k],
-                device_id=(e, lax.rem(t + k, m)),
-                device_id_type=MESH,
-            )
-            start([passed[d, k]])
+        to_far.append(pass_on(0, d, t, far))
+        to_near.append(pass_on(1, d, t, near))
     for load in loads[9:]:
         load.wait()
-    gate = jnp.zeros((tokens, egate_hbm.shape[2]), f32)
-    up = gate
-    for k in range(m):
-        q = lax.rem(t + m - k, m)
-        if k > 0:
-            for d in range(1, n):
-                passed[d, k].wait_recv()
+
+    def expand(q, gate, up):
         taken = a6[q].reshape(tokens, cols)
         at = pl.ds(pl.multiple_of(q * cols, cols), cols)
         gate = gate + jnp.dot(taken, egate_v[at, :], preferred_element_type=f32)
         up = up + jnp.dot(taken, eup_v[at, :], preferred_element_type=f32)
+        return gate, up
+
+    gate = jnp.zeros((tokens, egate_hbm.shape[2]), f32)
+    gate, up = expand(t, gate, gate)
+    for d in range(1, n):
+        to_far[d - 1].wait_recv()
+        relayed.append(pass_on(2, d, far, near))
+    gate, up = expand(far, gate, up)
+    for copy in to_near:
+        copy.wait_recv()
+    gate, up = expand(near, gate, up)
+    for copy in relayed:
+        copy.wait_recv()
+    gate, up = expand(cross, gate, up)
     gate = jnp.minimum(gate, clamp_limit)
     up = jnp.clip(up, -clamp_limit, clamp_limit)
     hidden = ((up + 1.0) * gate * jax.nn.sigmoid(gate_alpha * gate)).astype(bf16)
 
-    seventh = []
-    for k in [2, 3, 1, 0] if m == 4 else list(range(1, m)) + [0]:
-        q = lax.rem(t + k, m)
+    def partial_of(q):
         at = pl.ds(pl.multiple_of(q * cols, cols), cols)
-        part = jnp.dot(hidden, edown_v[:, at], preferred_element_type=f32).astype(bf16)
-        if k == 0:
-            own = part.astype(f32)
-        else:
-            s7[q] = part
-            seventh += start([tp_copy(1, k, s7.at[q], r7.at[t])])
-    for copy in seventh:
-        copy.wait_recv()
-    for k in range(1, m):
-        own = own + r7[lax.rem(t + k, m)].astype(f32)
+        return jnp.dot(hidden, edown_v[:, at], preferred_element_type=f32).astype(bf16)
+
+    def share(kind, source, target, place):
+        copy = pltpu.make_async_remote_copy(
+            src_ref=source,
+            dst_ref=place,
+            send_sem=fw_send.at[0, kind],
+            recv_sem=fw_recv.at[0, kind],
+            device_id=(e, target),
+            device_id_type=MESH,
+        )
+        return start([copy])[0]
+
+    s7[0] = partial_of(cross)
+    far_share = share(0, s7.at[0], near, r7.at[0])
+    s7[1] = partial_of(near)
+    own_share = share(1, s7.at[1], near, r7.at[1])
+    far_sum = partial_of(far).astype(f32)
+    far_share.wait_recv()
+    s7[2] = (far_sum + r7[0].astype(f32)).astype(bf16)
+    last_share = share(2, s7.at[2], far, r7.at[2])
+    own = partial_of(t).astype(f32)
+    own_share.wait_recv()
+    own = own + r7[1].astype(f32)
+    last_share.wait_recv()
+    own = own + r7[2].astype(f32)
     s8[...] = own.astype(bf16).reshape(n, seqs, cols)
     r8[e] = s8[e]
     eighth = start([ep_copy(5, d, s8.at[lax.rem(e + d, n)], r8.at[e]) for d in range(1, n)])
     named = routes[...]
     gates = route_gates[...]
+    same = lax.broadcasted_iota(jnp.int32, (seqs, seqs), 0) == lax.broadcasted_iota(
+        jnp.int32, (seqs, seqs), 1
+    )
+    weights = []
+    for j in range(n):
+        weight = jnp.sum(jnp.where(named == j, gates, 0.0), axis=0, keepdims=True)
+        weight = jnp.where(same, jnp.broadcast_to(weight, (seqs, seqs)), 0.0)
+        weights.append(jnp.sum(weight, axis=1, keepdims=True))
     for copy in eighth:
         copy.wait_recv()
     moe = jnp.zeros((seqs, cols), f32)
     for j in range(n):
-        weight = jnp.sum(jnp.where(named == j, gates, 0.0), axis=1, keepdims=True)
-        moe = moe + weight * r8[j].astype(f32)
-    a9[t] = moe
-    ninth = start([tp_copy(2, d, a9.at[t], a9.at[t]) for d in range(1, m)])
+        moe = moe + weights[j] * r8[j].astype(f32)
+    a9[t] = moe.astype(bf16)
+    ninth = start([tp_copy(1, d, a9.at[t], a9.at[t]) for d in range(1, m)])
     for copy in ninth:
         copy.wait_recv()
-    moe = jnp.concatenate([a9[q] for q in range(m)], axis=1)
+    moe = jnp.concatenate([a9[q] for q in range(m)], axis=1).astype(f32)
     layer_out[...] = (middle + row_scale(moe) * out_gain[...]).astype(bf16)
     for copy in sent:
         copy.wait_send()
@@ -537,7 +583,7 @@
     vmem = pl.BlockSpec(memory_space=pltpu.VMEM)
     hbm = pl.BlockSpec(memory_space=pl.ANY)
     dma = pltpu.SemaphoreType.DMA
-    return pl.pallas_call(
+    results = pl.pallas_call(
         functools.partial(layer_kernel, n, m),
         out_shape=(
             jax.ShapeDtypeStruct(layer_in.shape, bf16),
@@ -548,9 +594,9 @@
         scratch_shapes=[
             pltpu.VMEM(state_in.shape, f32),
             pltpu.VMEM((3, rows, cols), bf16),
-            pltpu.VMEM((width, low), bf16),
+            pltpu.VMEM((low, width), bf16),
             pltpu.VMEM((low, cols), bf16),
-            pltpu.VMEM((width, low), bf16),
+            pltpu.VMEM((low, width), bf16),
             pltpu.VMEM((low, cols), bf16),
             pltpu.VMEM(out_weight.shape, bf16),
             pltpu.VMEM((width, hidden), bf16),
@@ -569,11 +615,11 @@
             pltpu.VMEM((m, n, seqs, rows), bf16),
             pltpu.VMEM((m, seqs, cols), bf16),
             pltpu.VMEM((m, n, seqs, cols), bf16),
-            pltpu.VMEM((m, tokens, cols), bf16),
-            pltpu.VMEM((m, tokens, cols), bf16),
+            pltpu.VMEM((3, tokens, cols), bf16),
+            pltpu.VMEM((3, tokens, cols), bf16),
             pltpu.VMEM((n, seqs, cols), bf16),
             pltpu.VMEM((n, seqs, cols), bf16),
-            pltpu.VMEM((m, seqs, cols), f32),
+            pltpu.VMEM((m, seqs, cols), bf16),
             dma((13,)),
             dma((6, n)),
             dma((6, n)),
@@ -587,10 +633,44 @@
         ),
     )(
         layer_in, line(mix_gain), line(decay_base), line(rate_base), line(key_scale),
-        line(group_gain), line(post_gain), line(ffn_gain), line(out_gain), routes, route_gates,
-        state_in, rec_weight, key_weight, val_weight, decay_down, decay_up, rate_down, rate_up,
+        line(group_gain), line(post_gain), line(ffn_gain), line(out_gain), routes.T, route_gates.T,
+        state_in, rec_weight, key_weight, val_weight, decay_down.T, decay_up, rate_down.T, rate_up,
         out_weight, expert_gate, expert_up, expert_down,
     )
+    return pl.pallas_call(
+        hand_over,
+        out_shape=(
+            jax.ShapeDtypeStruct(layer_in.shape, bf16),
+            jax.ShapeDtypeStruct(state_in.shape, f32),
+        ),
+        in_specs=[hbm, hbm],
+        out_specs=(hbm, hbm),
+        scratch_shapes=[
+            pltpu.VMEM(layer_in.shape, bf16),
+            pltpu.VMEM(state_in.shape, f32),
+            dma((seqs + 1,)),
+            dma((seqs + 1,)),
+        ],
+        compiler_params=pltpu.CompilerParams(vmem_limit_bytes=60 * 1024 * 1024),
+    )(*results)
+
+
+def hand_over(token_in, state_in, token_out, state_out, token_v, state_v, in_sem, out_sem):
+    count = state_in.shape[0]
+    reads = [pltpu.make_async_copy(token_in, token_v, in_sem.at[count])]
+    writes = [pltpu.make_async_copy(token_v, token_out, out_sem.at[count])]
+    step = 2
+    for i in range(0, count, step):
+        at = pl.ds(i, step)
+        reads.append(pltpu.make_async_copy(state_in.at[at], state_v.at[at], in_sem.at[i]))
+        writes.append(pltpu.make_async_copy(state_v.at[at], state_out.at[at], out_sem.at[i]))
+    for copy in reads:
+        copy.start()
+    for read, write in zip(reads, writes):
+        read.wait()
+        write.start()
+    for copy in writes:
+        copy.wait()
 
 
 def choose(n, m, *args):
@@ -607,6 +687,8 @@
         and seqs % 16 == 0
         and heads % 8 == 0
         and cols * m == width
+        and m == 4
+        and args[1].shape[2] % (8 * HEAD_DIM) == 0
     ):
         return fused_local(n, m, *args)
     return local(*args)

time: 76.8 us -> 65.6 us (0.85)
  local copies, waits for them, and re-layouts: 11.2 us -> 0 us
    unnamed x6 -> x0, local copies, waits for them, and re-layouts: 11.2 us -> none
    pallas_call x0 -> x1, Pallas kernels: none -> 2.59 us  [fused_local(): pl.pallas_call(hand_over, out_shape=(jax.ShapeDtypeStruct(layer_in.shape,...]
    pallas_call x1, Pallas kernels: 64.6 us -> 62.2 us  [fused_local(): pl.pallas_call(functools.partial(layer_kernel, n, m), out_shape=(jax.Shap...]
where the time goes in v2:
time: 65.6 us; the launch traced here: 65.4 us
  Pallas kernels  64.8 us (99%)
    pallas_call x1, Pallas kernels, fused_local(): pl.pallas_call(functools.partial(layer_kernel, n, m), out_shape=(jax.Shap...  62.2 us
    pallas_call x1, Pallas kernels, fused_local(): pl.pallas_call(hand_over, out_shape=(jax.ShapeDtypeStruct(layer_in.shape,...  2.59 us

profile of v2, /device:TPU:0, one launch (start us, length us, event | category | flops | bytes accessed | tf_op | source)
XLA Modules:
  0.0 65.4 jit_solution(13272896378174819993)
XLA Ops:
  0.6 62.2 %shard_map.230 = (bf16[16,2048]{1,0:T(8,128)(2,1)}, f32[16,8,4096]{2,1,0:T(8,128)}) custom-call(bf16[16,2048]{1,0:T(8,128)(2,1)} %layer_in.1, f32[1,2048]{1,0:T(1,128)} %bitcast.14, f32[1,512]{1,0:T(1,128)} %bitcast.18, f32[1,512]{1,0:T(1,128)} %bitcast.19, f32[1,512]{1,0:T(1,128)} %bitcast.20, f32[1,512]{1,0:T(1,128)} %bitcast.21, f32[1,2048]{1,0:T(1,128)} %bitcast.15, ...), custom_call_target="tpu_custom_call" | custom-call | tf_op jit(solution)/shard_map/pallas_call | solution.py:586
  62.8 2.6 %shard_map.231 = (bf16[16,2048]{1,0:T(8,128)(2,1)}, f32[16,8,4096]{2,1,0:T(8,128)}) custom-call(bf16[16,2048]{1,0:T(8,128)(2,1)} %get-tuple-element.4.token_in, f32[16,8,4096]{2,1,0:T(8,128)} %get-tuple-element.5.state_in), custom_call_target="tpu_custom_call" | custom-call | tf_op jit(solution)/shard_map/pallas_call | solution.py:640
